TPU v7x, 512 devices: a whole 4x8x8 slice. The times are simulated.
512 devices in a mesh: sp: 128 (over z, y, core), tp: 4 (over x).
Axes of the slice: x: 4, y: 8, z: 8, core: 2. Of those that a mesh axis runs over, the one named last changes fastest.
Arguments:
- activations: bfloat16 [65536, 2048], P('sp', 'tp'), may hold values from -250 to 250
- norm_gain: bfloat16 [2048], P('tp'), may hold values from 0.099609375 to 1.8984375
- pool_weight: bfloat16 [2048, 1024], P('sp', 'tp'), may hold values from -0.125 to 0.125
- gate_weight: bfloat16 [2048, 1024], P('sp', 'tp'), may hold values from -0.125 to 0.125
- value_weight: bfloat16 [2048, 1024], P('sp', 'tp'), may hold values from -0.125 to 0.125
- key_weight: bfloat16 [2048, 256], P('sp', 'tp'), may hold values from -0.125 to 0.125
- read_weight: bfloat16 [2048, 256], P('sp', 'tp'), may hold values from -0.125 to 0.125
- step_weight: bfloat16 [2048, 16], P('sp', 'tp'), may hold values from -0.125 to 0.125
- pool_mix: bfloat16 [4, 256, 256], P('tp'), may hold values from -0.375 to 0.375
- pool_scale: float32 [1024], P('tp'), may hold values from 0.1 to 1.9
- taps_value: float32 [4, 1024], P(None, 'tp'), may hold values from -3 to 3
- taps_key: float32 [4, 256], P(None, 'tp'), may hold values from -3 to 3
- taps_read: float32 [4, 256], P(None, 'tp'), may hold values from -3 to 3
- step_bias: float32 [16], P('tp'), may hold values from -1 to 1
- decay_log: float32 [16], P('tp')
- decay_extra: float32 [65536, 16], P('sp', 'tp'), may hold values from -1 to 0
- skip_scale: float32 [16], P('tp'), may hold values from 0.5 to 2
- state_gain: float32 [1024], P('tp'), may hold values from 0.1 to 1.9
- out_pool_weight: bfloat16 [1024, 2048], P('tp', 'sp'), may hold values from -0.125 to 0.125
- out_state_weight: bfloat16 [1024, 2048], P('tp', 'sp'), may hold values from -0.125 to 0.125
Outputs:
- mixed: bfloat16 [65536, 2048], P('sp', 'tp')
All inputs are finite; a program needn't handle non-finite values.
Results may differ from a plain program's by a relative error of at most 0.007.
Values may be sent and summed in bfloat16 or wider, within the bound.
No kernel may reach another device: no remote copies, remote signals or barrier semaphores. Data moves between devices by JAX's collectives and lax.ppermute only.
A program may use at most 64 MiB of HBM per device.

v0:
```python
import jax
import jax.numpy as jnp
from jax import lax
from jax.sharding import Mesh
from jax.sharding import PartitionSpec as P

D = 2048
SSM_STATE = 64
POOL_GROUPS = 4
SCAN_BLOCK = 128
MIX_W = 1024
SP = ("sp_0", "sp_1", "sp_2")
EPSILON = 1e-06
HIGH = lax.Precision.HIGHEST


def sent_to_all(array, axis):
    copies = jnp.broadcast_to(array, (lax.axis_size(axis), *array.shape))
    return lax.all_to_all(copies, axis, split_axis=0, concat_axis=0, tiled=True)


def over_copies(array, axis):
    everything = sent_to_all(array, axis)
    return jnp.sum(everything, axis=0)


def laid_out(pieces, dim):
    pieces = jnp.moveaxis(pieces, 0, dim)
    shape = pieces.shape
    return pieces.reshape(*shape[:dim], shape[dim] * shape[dim + 1], *shape[dim + 2 :])


def collect(array, axis, dim):
    return laid_out(sent_to_all(array, axis), dim)


def shifted(value, axis, steps):
    count = lax.axis_size(axis)
    leading, last = (max(0, -steps), min(count, count - steps))
    return lax.ppermute(value, axis, [(source, source + steps) for source in range(leading, last)])


def neutral_like(array, identity):
    return jax.tree.map(
        lambda part, zero: jnp.zeros_like(part) + jnp.asarray(zero, part.dtype), array, identity
    )


def all_in_one(array, axis):
    leaves = jax.tree.leaves(array)
    order = sorted(range(len(leaves)), key=lambda k: -leaves[k].size)
    width = (1, *leaves[order[0]].shape)[-1]
    lines = [
        jnp.pad(leaves[k].reshape(-1), (0, -leaves[k].size % width)).reshape(-1, width)
        for k in order
    ]
    both, at, found = (lax.all_gather(jnp.concatenate(lines), axis), 0, {})
    for k, line in zip(order, lines):
        section = both[:, at : at + len(line)].reshape(len(both), -1)
        found[k] = section[:, : leaves[k].size].reshape(-1, *leaves[k].shape)
        at += len(line)
    numbers = iter(range(len(leaves)))
    return jax.tree.map(lambda _: found[next(numbers)], array)


def prefix_by_axis(array, axes, combine, identity):
    before = start = neutral_like(array, identity)
    running = array
    for axis in reversed(axes):
        count, place = (lax.axis_size(axis), lax.axis_index(axis))
        pieces = all_in_one(running, axis)
        inside, running = (start, start)
        for k in range(count):
            passed = k < place
            running = combine(running, jax.tree.map(lambda part: part[k], pieces))
            inside = jax.tree.map(lambda new, old: jnp.where(passed, new, old), running, inside)
        before = combine(inside, before)
    return before


def split_up(array, dim, count):
    before, after = (array.shape[:dim], array.shape[dim + 1 :])
    return jnp.moveaxis(array.reshape(*before, count, -1, *after), dim, 0)


def summed_on_arrival(array, axis, dim):
    pieces = split_up(array, dim, lax.axis_size(axis))
    arrived = lax.all_to_all(pieces, axis, split_axis=0, concat_axis=0, tiled=True)
    return arrived.astype(jnp.float32).sum(axis=0)


def backward_kernel(extended, taps):
    width = taps.shape[0]
    length = extended.shape[0] - (width - 1)
    widened_rows = extended.astype(jnp.float32)
    total = jnp.zeros((length, extended.shape[1]), jnp.float32)
    for offset in range(width):
        total = total + taps[offset][None, :] * widened_rows[offset : offset + length]
    return jax.nn.silu(total).astype(jnp.bfloat16)


def combine_states(preceding_token, later):
    return (preceding_token[0] * later[0], preceding_token[1] * later[0][:, None, None] + later[1])


def local(
    activations,
    norm_gain,
    pool_weight,
    gate_weight,
    value_weight,
    key_weight,
    read_weight,
    step_weight,
    pool_mix,
    pool_scale,
    taps_value,
    taps_key,
    taps_read,
    step_bias,
    decay_log,
    decay_extra,
    skip_scale,
    state_gain,
    out_pool_weight,
    out_state_weight,
):
    length = activations.shape[0]
    cluster_span = pool_weight.shape[1]
    local_mix = gate_weight.shape[1]
    local_state = key_weight.shape[1]
    local_heads = step_weight.shape[1]
    joined = jnp.concatenate(
        [pool_weight, gate_weight, value_weight, key_weight, read_weight, step_weight], axis=1
    )
    in_weight = lax.all_gather(joined, SP, axis=0, tiled=True)
    values = activations.astype(jnp.float32)
    squares = over_copies(jnp.sum(values * values, axis=-1), "tp")
    normed = (
        values * lax.rsqrt(squares / D + EPSILON)[:, None] * norm_gain.astype(jnp.float32)
    ).astype(jnp.bfloat16)
    projected = jnp.dot(collect(normed, "tp", 1), in_weight, preferred_element_type=jnp.float32)
    column = 0
    pool_in = projected[:, column : column + cluster_span].astype(jnp.bfloat16)
    column = column + cluster_span
    gate_in = projected[:, column : column + local_mix].astype(jnp.bfloat16)
    column = column + local_mix
    raw_value = projected[:, column : column + local_mix].astype(jnp.bfloat16)
    column = column + local_mix
    raw_key = projected[:, column : column + local_state].astype(jnp.bfloat16)
    column = column + local_state
    raw_read = projected[:, column : column + local_state].astype(jnp.bfloat16)
    column = column + local_state
    step_raw = projected[:, column : column + local_heads]
    raw_joined = jnp.concatenate([raw_value, raw_key, raw_read], axis=1)
    reach = 2**POOL_GROUPS - 1
    width = taps_value.shape[0]
    prior_pool, prior_joined = shifted(
        (pool_in[length - reach :], raw_joined[length - width + 1 :]), SP, 1
    )
    group = lax.axis_index("tp")
    running = jnp.concatenate([prior_pool, pool_in], axis=0).astype(jnp.float32)
    levels = []
    for level in range(POOL_GROUPS):
        stride = 2**level
        running = running[stride:] + running[:-stride]
        levels.append(running[running.shape[0] - length :])
    window_sum = lax.dynamic_index_in_dim(jnp.stack(levels), group, 0, keepdims=False)
    window = jnp.exp2((group + 1).astype(jnp.float32))
    position = (lax.axis_index(SP) * length + jnp.arange(length, dtype=jnp.int32)).astype(
        jnp.float32
    )
    counts = jnp.minimum(position + 1.0, window)
    pooled = (window_sum / counts[:, None] - pool_in.astype(jnp.float32)).astype(jnp.bfloat16)
    pool_out = (
        jnp.dot(pooled, pool_mix[0], preferred_element_type=jnp.float32) * pool_scale
    ).astype(jnp.bfloat16)
    all_taps = jnp.concatenate([taps_value, taps_key, taps_read], axis=1)
    convolved = backward_kernel(jnp.concatenate([prior_joined, raw_joined], axis=0), all_taps)
    head_value = convolved[:, :local_mix]
    key_vectors = convolved[:, local_mix : local_mix + local_state]
    read_vectors = convolved[:, local_mix + local_state :]
    head_dim = local_mix // local_heads
    groups_here = local_state // SSM_STATE
    repeat = local_heads // groups_here
    blocks = length // SCAN_BLOCK
    step_size = jax.nn.softplus(step_raw + step_bias)
    log_decay = -jnp.exp(decay_log) * step_size + decay_extra
    value_heads = head_value.astype(jnp.float32).reshape(length, local_heads, head_dim)
    value_blocks = value_heads.reshape(blocks, SCAN_BLOCK, local_heads, head_dim)
    key_blocks = jnp.repeat(
        key_vectors.astype(jnp.float32).reshape(length, groups_here, SSM_STATE), repeat, axis=1
    ).reshape(blocks, SCAN_BLOCK, local_heads, SSM_STATE)
    read_blocks = jnp.repeat(
        read_vectors.astype(jnp.float32).reshape(length, groups_here, SSM_STATE), repeat, axis=1
    ).reshape(blocks, SCAN_BLOCK, local_heads, SSM_STATE)
    step_blocks = step_size.reshape(blocks, SCAN_BLOCK, local_heads)
    running_decay = jnp.cumsum(log_decay.reshape(blocks, SCAN_BLOCK, local_heads), axis=1)
    lower = jnp.arange(SCAN_BLOCK)[:, None] >= jnp.arange(SCAN_BLOCK)[None, :]
    gaps = jnp.where(
        lower[None, :, :, None],
        running_decay[:, :, None, :] - running_decay[:, None, :, :],
        -jnp.inf,
    )
    weights = jnp.einsum("blhn,bshn->blsh", read_blocks, key_blocks, precision=HIGH) * jnp.exp(gaps)
    scaled_value = value_blocks * step_blocks[..., None]
    inner = jnp.einsum("blsh,bshp->blhp", weights, scaled_value, precision=HIGH)
    block_ends = running_decay[:, -1, :]
    trailing = jnp.exp(block_ends[:, None, :] - running_decay)
    fresh = jnp.einsum("bshn,bsh,bshp->bhpn", key_blocks, trailing, scaled_value, precision=HIGH)

    def advance(carry, inputs):
        block_decay, block_state = inputs
        return (carry * block_decay[:, None, None] + block_state, carry)

    local_total, prefix = lax.scan(
        advance,
        jnp.zeros((local_heads, head_dim, SSM_STATE), jnp.float32),
        (jnp.exp(block_ends), fresh),
    )
    offsets = jnp.cumsum(block_ends, axis=0) - block_ends
    device_decay = jnp.exp(offsets[-1] + block_ends[-1])
    incoming_decay, incoming = prefix_by_axis(
        (device_decay, local_total),
        SP,
        combine_states,
        (jnp.ones_like(device_decay), jnp.zeros_like(local_total)),
    )
    from_device = running_decay + offsets[:, None, :]
    local_off = (
        jnp.einsum("blhn,bhpn->blhp", read_blocks, prefix, precision=HIGH)
        * jnp.exp(running_decay)[..., None]
    )
    far_off = (
        jnp.einsum("blhn,hpn->blhp", read_blocks, incoming, precision=HIGH)
        * jnp.exp(from_device)[..., None]
    )
    scan_out = (inner + local_off + far_off).reshape(length, local_heads, head_dim) + skip_scale[
        None, :, None
    ] * value_heads
    gated = scan_out.reshape(length, local_mix) * jax.nn.silu(gate_in.astype(jnp.float32))
    gate_squares = over_copies(jnp.sum(gated * gated, axis=-1), "tp")
    state_out = (gated * lax.rsqrt(gate_squares / MIX_W + EPSILON)[:, None] * state_gain).astype(
        jnp.bfloat16
    )
    branch_rows = jnp.concatenate([pool_out, state_out], axis=1)
    out_weight = jnp.concatenate([out_pool_weight, out_state_weight], axis=0)
    terms = jnp.dot(
        branch_rows,
        lax.all_gather(out_weight, SP, axis=1, tiled=True),
        preferred_element_type=jnp.float32,
    )
    result = summed_on_arrival(terms.astype(jnp.bfloat16), "tp", 1)
    return result.astype(jnp.bfloat16)


def solution(mesh):
    torus = Mesh(mesh.devices.reshape(8, 8, 2, mesh.shape["tp"]), ("sp_0", "sp_1", "sp_2", "tp"))
    placed = (
        P(SP, "tp"),
        P("tp"),
        P(SP, "tp"),
        P(SP, "tp"),
        P(SP, "tp"),
        P(SP, "tp"),
        P(SP, "tp"),
        P(SP, "tp"),
        P("tp", None, None),
        P("tp"),
        P(None, "tp"),
        P(None, "tp"),
        P(None, "tp"),
        P("tp"),
        P("tp"),
        P(SP, "tp"),
        P("tp"),
        P("tp"),
        P("tp", SP),
        P("tp", SP),
    )
    return jax.shard_map(local, mesh=torus, in_specs=placed, out_specs=P(SP, "tp"), check_vma=False)
```

profile of v0, /device:TPU:24, one launch (start us, length us, event | category | flops | bytes accessed | tf_op | source)
XLA Modules:
  0.0 253.4 jit_solution(12574823793756148212)
XLA Ops:
  6.5 0.8 copy.224
  7.3 1.5 concatenate.30
  8.8 1.2 fusion.7
  10.0 0.6 broadcast_in_dim.62
  10.6 4.3 %all-to-all-start = ((f32[4,1,512]{2,1,0:T(1,128)}), f32[4,1,512]{2,1,0:T(1,128)S(1)}, u32[]{:S(2)}, u32[]{:S(2)}) async-start(f32[4,1,512]{2,1,0:T(1,128)} %broadcast_in_dim.62), calls=%async_computation | async-start | bytes 16384 | tf_op jit(solution)/shard_map/all_to_all | solution.py:19
  14.9 0.7 convert_element_type.63
  15.6 4.6 %all-to-all-done = f32[4,1,512]{2,1,0:T(1,128)S(1)} async-done(((f32[4,1,512]{2,1,0:T(1,128)}), f32[4,1,512]{2,1,0:T(1,128)S(1)}, u32[]{:S(2)}, u32[]{:S(2)}) %all-to-all-start) | async-done | bytes 8224 | tf_op jit(solution)/shard_map/all_to_all | solution.py:19
  20.3 1.2 fusion.9
  21.7 1.6 broadcast_in_dim.63
  23.4 3.8 %all-to-all-start.1 = ((bf16[4,512,512]{1,2,0:T(8,128)(2,1)}), bf16[4,512,512]{1,2,0:T(8,128)(2,1)S(1)}, u32[]{:S(2)}, u32[]{:S(2)}) async-start(bf16[4,512,512]{1,2,0:T(8,128)(2,1)} %broadcast_in_dim.63), calls=%async_computation.1 | async-start | bytes 4194304 | tf_op jit(solution)/shard_map/all_to_all | solution.py:19
  28.0 0.7 mul.636
  29.4 0.6 iota_compare_fusion
  30.0 0.6 slice_reduce_fusion.4
  30.6 21.7 %all-to-all-done.1 = bf16[4,512,512]{1,2,0:T(8,128)(2,1)S(1)} async-done(((bf16[4,512,512]{1,2,0:T(8,128)(2,1)}), bf16[4,512,512]{1,2,0:T(8,128)(2,1)S(1)}, u32[]{:S(2)}, u32[]{:S(2)}) %all-to-all-start.1) | async-done | bytes 2097184 | tf_op jit(solution)/shard_map/all_to_all | solution.py:19
  52.3 46.8 %all-gather.9.cloned.1.call-done = bf16[2048,900]{1,0:T(8,128)(2,1)} async-done(((bf16[16,900]{1,0:T(8,128)(2,1)}), bf16[2048,900]{1,0:T(8,128)(2,1)}) %all-gather.9.cloned.1.call-update) | async-done | bytes 3686416 | tf_op jit(solution)/shard_map/all_gather | solution.py:136
  99.1 4.4 %fusion.160 = (bf16[512,900]{0,1:T(8,128)(2,1)S(1)}, f32[512,900]{0,1:T(8,128)S(1)}) fusion(bf16[512,2048]{0,1:T(8,128)(2,1)S(1)} %bitcast.291, bf16[2048,900]{1,0:T(8,128)(2,1)} %all-gather.9.cloned.1.call-done), kind=kOutput, calls=%fused_computation.265 | convolution fusion | flops 1887897600 | bytes 8548352 | tf_op jit(solution)/shard_map/dot_general | solution.py:142
  104.3 2.1 collective-permute-start.1
  106.5 0.7 copy.230
  107.2 0.7 slice.355
  108.2 0.7 copy.260
  108.9 0.7 copy.234
  109.6 3.6 %collective-permute-start = (bf16[15,256]{0,1:T(8,128)(2,1)}, bf16[15,256]{0,1:T(8,128)(2,1)}, u32[]{:S(2)}, u32[]{:S(2)}) collective-permute-start(bf16[15,256]{0,1:T(8,128)(2,1)} %slice.355), channel_id=1, source_target_pairs={{0,4},{4,8},{8,12},{12,16},{16,20},{20,24},{24,28},{28,32},{32,36}... | collective-permute-start | bytes 23048 | tf_op jit(solution)/shard_map/ppermute | solution.py:40
  113.5 0.9 multiply_convert_fusion
  114.4 0.7 convert_bitcast_fusion.1
  115.4 0.9 fusion.27
  116.3 3.1 %while.13 = (s32[]{:T(128)}, f32[4,64,64]{2,1,0:T(8,128)S(1)}, f32[4,4,64,64]{3,2,1,0:T(8,128)}, f32[4,4]{1,0:T(4,128)S(1)}, f32[4,4,64,64]{3,2,1,0:T(8,128)S(1)}, /*index=5*/s32[]{:T(128)}, s32[]{:T(128)}) while((s32[]{:T(128)}, f32[4,64,64]{2,1,0:T(8,128)S(1)}, f32[4,4,64,64]{3,2,1,0:T(8,128)}, f32[4,4]{1,0:T(4,128)S(1)}, ...), condition=%wide.region_4.5_spmd.clone, body=%wide.region_3.4_spmd.clone.sunk | while | flops 65539 | bytes 393872 | solution.py:216
  116.3 0.7 bitcast_dynamic-update-slice_fusion.2
  117.1 0.7 bitcast_dynamic-update-slice_fusion.2
  117.9 0.7 bitcast_dynamic-update-slice_fusion.2
  118.7 0.7 bitcast_dynamic-update-slice_fusion.2
  119.6 1.9 all-gather.3
  122.5 26.2 %all-gather.4 = f32[8,257,64]{1,2,0:T(8,128)S(1)} all-gather(f32[1,257,64]{1,2,0:T(8,128)S(1)} %maximum_bitcast_fusion.1), channel_id=3, replica_groups=mesh['sp_0'=8,'sp_1'=8,'sp_2'=2,'tp'=4] {'sp_1'}, dimensions={0}, use_global_device_ids=true | all-gather | bytes 592128 | tf_op jit(solution)/shard_map/all_gather | solution.py:57
  150.9 27.0 %all-gather.5 = f32[8,257,64]{1,2,0:T(8,128)S(1)} all-gather(f32[1,257,64]{1,2,0:T(8,128)S(1)} %maximum_bitcast_fusion.2), channel_id=4, replica_groups=mesh['sp_0'=8,'sp_1'=8,'sp_2'=2,'tp'=4] {'sp_0'}, dimensions={0}, use_global_device_ids=true | all-gather | bytes 592128 | tf_op jit(solution)/shard_map/all_gather | solution.py:57
  177.9 0.8 fusion.155
  178.7 1.6 copy.267
  180.3 1.6 copy.268
  181.9 1.6 copy.269
  183.5 1.6 copy.270
  185.1 1.6 copy.271
  186.7 1.6 copy.272
  188.3 1.6 copy.273
  189.9 0.8 copy.274
  190.6 0.7 copy.288
  191.3 0.8 fusion.156
  192.1 1.6 copy.275
  193.7 1.6 copy.276
  195.3 1.6 copy.277
  196.9 0.8 copy.278
  197.6 0.8 copy.279
  198.4 1.6 copy.280
  200.0 1.6 copy.281
  201.6 0.8 copy.282
  202.4 0.8 copy.283
  203.2 0.8 copy.284
  204.0 1.7 fusion.4
  205.7 2.8 %fusion.1 = f32[4,128,128,4]{1,2,3,0:T(8,128)S(1)} fusion(f32[4,128,4]{1,2,0:T(4,128)} %copy.230, pred[128,128]{0,1:T(8,128)(4,1)} %iota_compare_fusion, f32[4,128,64]{1,2,0:T(8,128)S(1)} %bitcast.295, f32[4,128,64]{1,2,0:T(8,128)S(1)} %bitcast.299), kind=kOutput, calls=%fused_computation.11 | convolution fusion | flops 202113024 | bytes 1335296 | tf_op jit(solution)/shard_map/blhn,bshn->blsh/dot_general | solution.py:205
  208.6 2.4 fusion.5
  211.1 1.1 fusion.3
  213.4 4.3 %all-to-all-start.2 = ((f32[4,1,512]{2,1,0:T(1,128)}), f32[4,1,512]{2,1,0:T(1,128)S(1)}, u32[]{:S(2)}, u32[]{:S(2)}) async-start(f32[4,1,512]{2,1,0:T(1,128)} %broadcast_in_dim.73), calls=%async_computation.2 | async-start | bytes 16384 | tf_op jit(solution)/shard_map/all_to_all | solution.py:19
  217.7 1.0 maximum_convert_fusion.1
  220.5 2.5 all-to-all-done.2
  223.2 2.9 %convolution_convert_fusion = bf16[512,2048]{1,0:T(8,128)(2,1)S(1)} fusion(bf16[512,2048]{0,1:T(8,128)(2,1)} %all-gather.11.cloned.1.call-done, bf16[512,256]{0,1:T(8,128)(2,1)S(1)} %multiply_convert_fusion.1, bf16[512,256]{0,1:T(8,128)(2,1)S(1)} %fusion.6), kind=kOutput, calls=%fused_computation.4 | convolution fusion | flops 1075838976 | bytes 4718592 | tf_op jit(solution)/shard_map/dot_general | solution.py:248
  226.3 19.0 %all_to_all.22 = bf16[4,512,512]{2,1,0:T(8,128)(2,1)S(1)} all-to-all(bf16[4,512,512]{2,1,0:T(8,128)(2,1)S(1)} %bitcast.290), channel_id=1, replica_groups=mesh['sp_0'=8,'sp_1'=8,'sp_2'=2,'tp'=4] {'tp'}, dimensions={0} | all-to-all | bytes 4194304 | tf_op jit(solution)/shard_map/all_to_all | solution.py:88
  245.3 1.2 reduce_sum.52
  (177 shorter events, 10.1 us)
Async XLA Ops:
  6.5 213.4 %copy-start = (bf16[1,256,256]{2,1,0:T(8,128)(2,1)S(1)}, bf16[1,256,256]{2,1,0:T(8,128)(2,1)}, u32[]{:S(2)}) copy-start(bf16[1,256,256]{2,1,0:T(8,128)(2,1)} %param.30) | copy-start | bytes 393220
  6.5 92.5 %all-gather.9.cloned.1.call-start = ((), (), s32[]{:S(2)}) async-start(), calls=%async_computation.4 | async-start | bytes 4227072 | tf_op jit(solution)/shard_map/all_gather | solution.py:136
  10.6 9.6 %all-to-all-start = ((f32[4,1,512]{2,1,0:T(1,128)}), f32[4,1,512]{2,1,0:T(1,128)S(1)}, u32[]{:S(2)}, u32[]{:S(2)}) async-start(f32[4,1,512]{2,1,0:T(1,128)} %broadcast_in_dim.62), calls=%async_computation | async-start | bytes 16384 | tf_op jit(solution)/shard_map/all_to_all | solution.py:19
  23.3 3.9 %copy-start.15 = (bf16[256,16]{0,1:T(8,128)(2,1)S(1)}, bf16[256,16]{0,1:T(8,128)(2,1)}, u32[]{:S(2)}) copy-start(bf16[256,16]{0,1:T(8,128)(2,1)} %param.41) | copy-start | bytes 24580
  23.3 3.9 %copy-start.16 = (bf16[256,16]{0,1:T(8,128)(2,1)S(1)}, bf16[256,16]{0,1:T(8,128)(2,1)}, u32[]{:S(2)}) copy-start(bf16[256,16]{0,1:T(8,128)(2,1)} %param.40) | copy-start | bytes 24580
  23.3 4.6 %copy-start.36 = (f32[4]{0:T(128)S(1)}, f32[4]{0:T(128)}, u32[]{:S(2)}) copy-start(f32[4]{0:T(128)} %param.38) | copy-start | bytes 52
  23.3 6.0 %copy-start.26 = (f32[4,256]{1,0:T(4,128)S(1)}, f32[4,256]{1,0:T(4,128)}, u32[]{:S(2)}) copy-start(f32[4,256]{1,0:T(4,128)} %param.32) | copy-start | bytes 12292
  23.3 6.0 %copy-start.30 = (f32[4,64]{1,0:T(4,128)S(1)}, f32[4,64]{1,0:T(4,128)}, u32[]{:S(2)}) copy-start(f32[4,64]{1,0:T(4,128)} %param.34) | copy-start | bytes 3076
  23.3 5.9 %copy-start.31 = (f32[4,64]{1,0:T(4,128)S(1)}, f32[4,64]{1,0:T(4,128)}, u32[]{:S(2)}) copy-start(f32[4,64]{1,0:T(4,128)} %param.33) | copy-start | bytes 3076
  23.3 7.2 %copy-start.38 = (f32[4]{0:T(128)S(1)}, f32[4]{0:T(128)}, u32[]{:S(2)}) copy-start(f32[4]{0:T(128)} %param.36) | copy-start | bytes 52
  23.4 28.9 %all-to-all-start.1 = ((bf16[4,512,512]{1,2,0:T(8,128)(2,1)}), bf16[4,512,512]{1,2,0:T(8,128)(2,1)S(1)}, u32[]{:S(2)}, u32[]{:S(2)}) async-start(bf16[4,512,512]{1,2,0:T(8,128)(2,1)} %broadcast_in_dim.63), calls=%async_computation.1 | async-start | bytes 4194304 | tf_op jit(solution)/shard_map/all_to_all | solution.py:19
  27.1 196.1 %all-gather.11.cloned.1.call-start = ((), (), s32[]{:S(2)}) async-start(), calls=%async_computation.5 | async-start | bytes 2113536 | tf_op jit(solution)/shard_map/all_gather | solution.py:250
  99.1 4.4 %copy-start.17 = (f32[512,4]{0,1:T(4,128)S(1)}, f32[512,4]{0,1:T(4,128)}, u32[]{:S(2)}) copy-start(f32[512,4]{0,1:T(4,128)} %param.37) | copy-start | bytes 24580
  99.1 4.4 %copy-start.35 = (f32[4]{0:T(128)S(1)}, f32[4]{0:T(128)}, u32[]{:S(2)}) copy-start(f32[4]{0:T(128)} %param.35) | copy-start | bytes 52
  104.2 9.2 %copy-start.11 = (f32[384]{0:T(512)S(1)}, f32[384]{0:T(512)}, u32[]{:S(2)}) copy-start(f32[384]{0:T(512)} %get-tuple-element.53) | copy-start | bytes 4612
  104.2 9.2 %copy-start.12 = (f32[384]{0:T(512)S(1)}, f32[384]{0:T(512)}, u32[]{:S(2)}) copy-start(f32[384]{0:T(512)} %get-tuple-element.54) | copy-start | bytes 4612
  104.2 9.2 %copy-start.13 = (f32[384]{0:T(512)S(1)}, f32[384]{0:T(512)}, u32[]{:S(2)}) copy-start(f32[384]{0:T(512)} %get-tuple-element.55) | copy-start | bytes 4612
  104.2 9.2 %copy-start.14 = (f32[384]{0:T(512)S(1)}, f32[384]{0:T(512)}, u32[]{:S(2)}) copy-start(f32[384]{0:T(512)} %get-tuple-element.56) | copy-start | bytes 4612
  104.3 8.9 %collective-permute-start.1 = (bf16[3,384]{0,1:T(8,128)(2,1)S(1)}, bf16[3,384]{0,1:T(8,128)(2,1)S(1)}, u32[]{:S(2)}, u32[]{:S(2)}) collective-permute-start(bf16[3,384]{0,1:T(8,128)(2,1)S(1)} %slice.368), channel_id=1, source_target_pairs={{0,4},{4,8},{8,12},{12,16},{16,20},{20,24},{24,28},{28,32},{32,36}... | collective-permute-start | bytes 6920 | tf_op jit(solution)/shard_map/ppermute | solution.py:40
  109.6 108.1 %collective-permute-start = (bf16[15,256]{0,1:T(8,128)(2,1)}, bf16[15,256]{0,1:T(8,128)(2,1)}, u32[]{:S(2)}, u32[]{:S(2)}) collective-permute-start(bf16[15,256]{0,1:T(8,128)(2,1)} %slice.355), channel_id=1, source_target_pairs={{0,4},{4,8},{8,12},{12,16},{16,20},{20,24},{24,28},{28,32},{32,36}... | collective-permute-start | bytes 23048 | tf_op jit(solution)/shard_map/ppermute | solution.py:40
  115.2 1.1 copy-start.1
  121.6 27.2 %copy-start.25 = (f32[4]{0:T(128)}, f32[4]{0:T(128)S(1)}, u32[]{:S(2)}) copy-start(f32[4]{0:T(128)S(1)} %get-tuple-element.116) | copy-start | bytes 52
  121.6 27.2 %copy-start.33 = (f32[4]{0:T(128)}, f32[4]{0:T(128)S(1)}, u32[]{:S(2)}) copy-start(f32[4]{0:T(128)S(1)} %get-tuple-element.117) | copy-start | bytes 52
  121.6 0.6 copy-start.28
  148.9 2.0 copy-start.18
  148.9 2.0 copy-start.19
  148.9 2.0 copy-start.20
  148.9 2.0 copy-start.21
  148.9 2.0 copy-start.22
  148.9 2.0 copy-start.23
  148.9 2.0 copy-start.24
  148.9 1.1 copy-start.29
  191.3 12.6 %copy-start.3 = (f32[8,4,8,128]{3,2,1,0:T(8,128)S(1)}, f32[8,4,8,128]{3,2,1,0:T(8,128)}, u32[]{:S(2)}) copy-start(f32[8,4,8,128]{3,2,1,0:T(8,128)} %get-tuple-element.93) | copy-start | bytes 393220
  192.1 11.9 %copy-start.10 = (f32[8,1,64]{2,0,1:T(8,128)S(1)}, f32[8,1,64]{2,0,1:T(8,128)}, u32[]{:S(2)}) copy-start(f32[8,1,64]{2,0,1:T(8,128)} %copy.288) | copy-start | bytes 6148
  192.1 13.6 %copy-start.2 = (f32[8,4,8,128]{3,2,0,1:T(8,128)S(1)}, f32[8,4,8,128]{3,2,0,1:T(8,128)}, u32[]{:S(2)}) copy-start(f32[8,4,8,128]{3,2,0,1:T(8,128)} %copy-done.1) | copy-start | bytes 393220
  198.4 10.1 %copy-start.4 = (f32[1,256,64]{2,1,0:T(8,128)S(1)}, f32[1,256,64]{2,1,0:T(8,128)}, u32[]{:S(2)}) copy-start(f32[1,256,64]{2,1,0:T(8,128)} %copy.267) | copy-start | bytes 196612
  202.4 6.1 %copy-start.5 = (f32[1,256,64]{2,1,0:T(8,128)S(1)}, f32[1,256,64]{2,1,0:T(8,128)}, u32[]{:S(2)}) copy-start(f32[1,256,64]{2,1,0:T(8,128)} %copy.280) | copy-start | bytes 196612
  203.9 4.6 %copy-start.6 = (f32[1,256,64]{2,1,0:T(8,128)S(1)}, f32[1,256,64]{2,1,0:T(8,128)}, u32[]{:S(2)}) copy-start(f32[1,256,64]{2,1,0:T(8,128)} %copy.281) | copy-start | bytes 196612
  203.9 4.6 %copy-start.7 = (f32[1,256,64]{2,1,0:T(8,128)S(1)}, f32[1,256,64]{2,1,0:T(8,128)}, u32[]{:S(2)}) copy-start(f32[1,256,64]{2,1,0:T(8,128)} %copy.282) | copy-start | bytes 196612
  203.9 4.6 %copy-start.8 = (f32[1,256,64]{2,1,0:T(8,128)S(1)}, f32[1,256,64]{2,1,0:T(8,128)}, u32[]{:S(2)}) copy-start(f32[1,256,64]{2,1,0:T(8,128)} %copy.283) | copy-start | bytes 196612
  203.9 4.7 %copy-start.9 = (f32[1,256,64]{2,1,0:T(8,128)S(1)}, f32[1,256,64]{2,1,0:T(8,128)}, u32[]{:S(2)}) copy-start(f32[1,256,64]{2,1,0:T(8,128)} %copy.284) | copy-start | bytes 196612
  211.0 1.5 copy-start.27
  213.4 9.7 %all-to-all-start.2 = ((f32[4,1,512]{2,1,0:T(1,128)}), f32[4,1,512]{2,1,0:T(1,128)S(1)}, u32[]{:S(2)}, u32[]{:S(2)}) async-start(f32[4,1,512]{2,1,0:T(1,128)} %broadcast_in_dim.73), calls=%async_computation.2 | async-start | bytes 16384 | tf_op jit(solution)/shard_map/all_to_all | solution.py:19
  219.4 0.6 copy-start.32
  219.4 0.7 copy-start.37
  220.0 3.1 %copy-start.34 = (f32[256]{0:T(256)S(1)}, f32[256]{0:T(256)}, u32[]{:S(2)}) copy-start(f32[256]{0:T(256)} %param.39) | copy-start | bytes 3076
Sparse Core Ops, SparseCore 0:
  10.5 88.5 all-gather.8
  102.2 80.5 all-gather.10
where the time goes:
time: 255 us; the launch traced here: 253 us
  waiting for transfers between devices  75.8 us (30%)
  blocking collectives  74.1 us (29%)
  local copies, waits for them, and re-layouts  39.7 us (16%)
  starting transfers between devices  18.1 us (7%)
  matrix products  16.7 us (7%)
  other arithmetic  14.6 us (6%)
  between operations  14.4 us (6%)
    all_gather x3, blocking collectives, all_in_one(): both, at, found = (lax.all_gather(jnp.concatenate(lines), axis), 0, {})  55.1 us
    all_gather x1, waiting for transfers between devices, local(): in_weight = lax.all_gather(joined, SP, axis=0, tiled=True)  46.8 us
    all_to_all x3, waiting for transfers between devices, sent_to_all(): return lax.all_to_all(copies, axis, split_axis=0, concat_axis=0, tiled=True)  28.8 us
    squeeze x18, local copies, waits for them, and re-layouts, prefix_by_axis(): running = combine(running, jax.tree.map(lambda part: part[k], pieces))  23.7 us
    all_to_all x1, blocking collectives, summed_on_arrival(): lax.all_to_all(pieces, axis, split_axis=0, concat_axis=0, tiled=True)  19 us
    all_to_all x3, starting transfers between devices, sent_to_all(): return lax.all_to_all(copies, axis, split_axis=0, concat_axis=0, tiled=True)  12.3 us
    ppermute x2, starting transfers between devices, shifted(): lax.ppermute(value, axis, [(source, source + steps) for source in range(l...  5.72 us
  transfers between devices with their start and end apart: 7, of which 4 were waited for; matrix products, arithmetic and copies ran while one was open for 25% of the time, Pallas kernels for 0%

commit v1 on v0

--- a/solution.py
+++ b/solution.py
@@ -133,7 +133,10 @@
     joined = jnp.concatenate(
         [pool_weight, gate_weight, value_weight, key_weight, read_weight, step_weight], axis=1
     )
-    in_weight = lax.all_gather(joined, SP, axis=0, tiled=True)
+    size = lax.axis_size(SP)
+    parts = jnp.stack([joined for _ in range(size)])
+    parts = lax.all_to_all(parts, SP, split_axis=0, concat_axis=0)
+    in_weight = jnp.concatenate(parts, axis=0)
     values = activations.astype(jnp.float32)
     squares = over_copies(jnp.sum(values * values, axis=-1), "tp")
     normed = (

time: 255 us -> 329 us (1.29)
  the two profiles are of different devices: /device:TPU:24 before, /device:TPU:2 now
where the time goes in v1:
time: 329 us; the launch traced here: 327 us
  waiting for transfers between devices  117 us (36%)
  blocking collectives  77.1 us (23%)
  starting transfers between devices  46.5 us (14%)
  local copies, waits for them, and re-layouts  41.7 us (13%)
  other arithmetic  15.7 us (5%)
  matrix products  14.7 us (4%)
  between operations  14.7 us (4%)
    all_to_all x1, waiting for transfers between devices, local(): parts = lax.all_to_all(parts, SP, split_axis=0, concat_axis=0)  93.2 us
    all_gather x3, blocking collectives, all_in_one(): both, at, found = (lax.all_gather(jnp.concatenate(lines), axis), 0, {})  58.1 us
    squeeze x18, local copies, waits for them, and re-layouts, prefix_by_axis(): running = combine(running, jax.tree.map(lambda part: part[k], pieces))  24.6 us
    all_to_all x3, waiting for transfers between devices, sent_to_all(): return lax.all_to_all(copies, axis, split_axis=0, concat_axis=0, tiled=True)  23.5 us
    all_to_all x3, starting transfers between devices, sent_to_all(): return lax.all_to_all(copies, axis, split_axis=0, concat_axis=0, tiled=True)  20 us
    all_to_all x1, blocking collectives, summed_on_arrival(): lax.all_to_all(pieces, axis, split_axis=0, concat_axis=0, tiled=True)  19 us
    all_to_all x1, starting transfers between devices, local(): parts = lax.all_to_all(parts, SP, split_axis=0, concat_axis=0)  18.5 us
    ppermute x2, starting transfers between devices, shifted(): lax.ppermute(value, axis, [(source, source + steps) for source in range(l...  8.01 us
  transfers between devices with their start and end apart: 7, of which 4 were waited for; matrix products, arithmetic and copies ran while one was open for 18% of the time, Pallas kernels for 0%

profile of v1, /device:TPU:2, one launch (start us, length us, event | category | flops | bytes accessed | tf_op | source)
XLA Modules:
  0.0 327.3 jit_solution(6353807504458310868)
XLA Ops:
  6.5 1.3 fusion.7
  8.4 9.1 %all-to-all-start = ((f32[4,1,512]{2,1,0:T(1,128)}), f32[4,1,512]{2,1,0:T(1,128)S(1)}, u32[]{:S(2)}, u32[]{:S(2)}) async-start(f32[4,1,512]{2,1,0:T(1,128)} %broadcast_in_dim.62), calls=%async_computation | async-start | bytes 16384 | tf_op jit(solution)/shard_map/all_to_all | solution.py:19
  17.5 0.7 convert_element_type.63
  18.2 3.2 all-to-all-done
  21.4 1.2 fusion.9
  22.8 1.5 broadcast_in_dim.63
  24.4 5.2 %all-to-all-start.1 = ((bf16[4,512,512]{1,2,0:T(8,128)(2,1)}), bf16[4,512,512]{1,2,0:T(8,128)(2,1)S(1)}, u32[]{:S(2)}, u32[]{:S(2)}) async-start(bf16[4,512,512]{1,2,0:T(8,128)(2,1)} %broadcast_in_dim.63), calls=%async_computation.1 | async-start | bytes 4194304 | tf_op jit(solution)/shard_map/all_to_all | solution.py:19
  29.8 19.2 %all-to-all-done.1 = bf16[4,512,512]{1,2,0:T(8,128)(2,1)S(1)} async-done(((bf16[4,512,512]{1,2,0:T(8,128)(2,1)}), bf16[4,512,512]{1,2,0:T(8,128)(2,1)S(1)}, u32[]{:S(2)}, u32[]{:S(2)}) %all-to-all-start.1) | async-done | bytes 2097184 | tf_op jit(solution)/shard_map/all_to_all | solution.py:19
  49.0 2.5 stack.12
  51.6 18.5 %all-to-all-start.2 = ((bf16[128,16,900]{2,1,0:T(8,128)(2,1)}), bf16[128,16,900]{2,1,0:T(8,128)(2,1)}, u32[]{:S(2)}, u32[]{:S(2)}) async-start(bf16[128,16,900]{2,1,0:T(8,128)(2,1)} %stack.12), calls=%async_computation.2 | async-start | bytes 8388608 | tf_op jit(solution)/shard_map/all_to_all | solution.py:138
  71.0 0.6 mul.636
  72.4 0.6 iota_compare_fusion
  73.6 93.2 %all-to-all-done.2 = bf16[128,16,900]{2,1,0:T(8,128)(2,1)} async-done(((bf16[128,16,900]{2,1,0:T(8,128)(2,1)}), bf16[128,16,900]{2,1,0:T(8,128)(2,1)}, u32[]{:S(2)}, u32[]{:S(2)}) %all-to-all-start.2) | async-done | bytes 3686432 | tf_op jit(solution)/shard_map/all_to_all | solution.py:138
  166.8 4.4 %fusion.160 = (bf16[512,900]{0,1:T(8,128)(2,1)S(1)}, f32[512,900]{0,1:T(8,128)S(1)}) fusion(bf16[512,2048]{0,1:T(8,128)(2,1)S(1)} %bitcast.292, bf16[2048,900]{1,0:T(8,128)(2,1)} %bitcast.2), kind=kOutput, calls=%fused_computation.265 | convolution fusion | flops 1887897600 | bytes 8548352 | tf_op jit(solution)/shard_map/dot_general | solution.py:145
  172.0 1.3 collective-permute-start.1
  173.4 0.7 copy.230
  174.1 0.7 slice.355
  175.0 0.7 copy.260
  175.8 0.7 copy.234
  176.5 6.7 %collective-permute-start = (bf16[15,256]{0,1:T(8,128)(2,1)}, bf16[15,256]{0,1:T(8,128)(2,1)}, u32[]{:S(2)}, u32[]{:S(2)}) collective-permute-start(bf16[15,256]{0,1:T(8,128)(2,1)} %slice.355), channel_id=1, source_target_pairs={{0,4},{4,8},{8,12},{12,16},{16,20},{20,24},{24,28},{28,32},{32,36}... | collective-permute-start | bytes 23048 | tf_op jit(solution)/shard_map/ppermute | solution.py:40
  183.4 0.9 multiply_convert_fusion
  184.4 0.7 convert_bitcast_fusion.1
  185.4 0.9 fusion.27
  186.3 3.1 while.13
  186.3 0.7 bitcast_dynamic-update-slice_fusion.2
  187.1 0.7 bitcast_dynamic-update-slice_fusion.2
  187.9 0.7 bitcast_dynamic-update-slice_fusion.2
  188.7 0.7 bitcast_dynamic-update-slice_fusion.2
  189.6 1.9 all-gather.3
  192.4 27.9 %all-gather.4 = f32[8,257,64]{1,2,0:T(8,128)S(1)} all-gather(f32[1,257,64]{1,2,0:T(8,128)S(1)} %maximum_bitcast_fusion.1), channel_id=3, replica_groups=mesh['sp_0'=8,'sp_1'=8,'sp_2'=2,'tp'=4] {'sp_1'}, dimensions={0}, use_global_device_ids=true | all-gather | bytes 592128 | tf_op jit(solution)/shard_map/all_gather | solution.py:57
  222.6 28.2 %all-gather.5 = f32[8,257,64]{1,2,0:T(8,128)S(1)} all-gather(f32[1,257,64]{1,2,0:T(8,128)S(1)} %maximum_bitcast_fusion.2), channel_id=4, replica_groups=mesh['sp_0'=8,'sp_1'=8,'sp_2'=2,'tp'=4] {'sp_0'}, dimensions={0}, use_global_device_ids=true | all-gather | bytes 592128 | tf_op jit(solution)/shard_map/all_gather | solution.py:57
  250.9 0.8 fusion.155
  251.7 1.6 copy.267
  253.3 1.6 copy.268
  254.9 1.6 copy.269
  256.5 1.6 copy.270
  258.1 1.6 copy.271
  259.7 1.6 copy.272
  261.3 1.6 copy.273
  262.9 0.8 copy.274
  263.6 0.7 copy.288
  264.3 0.7 fusion.156
  265.1 1.7 copy.275
  266.8 1.6 copy.276
  268.3 1.6 copy.277
  269.9 0.8 copy.278
  270.7 0.7 copy.279
  271.4 1.6 copy.280
  273.1 1.6 copy.281
  274.7 0.7 copy.282
  275.4 0.6 fusion.158
  276.1 1.6 copy.283
  277.8 0.8 copy.284
  278.7 1.0 multiply_bitcast_fusion
  279.7 1.3 fusion.4
  281.0 2.8 fusion.1
  284.1 0.9 fusion.5
  285.0 1.1 fusion.3
  287.3 5.7 %all-to-all-start.3 = ((f32[4,1,512]{2,1,0:T(1,128)}), f32[4,1,512]{2,1,0:T(1,128)S(1)}, u32[]{:S(2)}, u32[]{:S(2)}) async-start(f32[4,1,512]{2,1,0:T(1,128)} %broadcast_in_dim.73), calls=%async_computation.3 | async-start | bytes 16384 | tf_op jit(solution)/shard_map/all_to_all | solution.py:19
  293.0 1.0 maximum_convert_fusion.1
  295.9 1.1 all-to-all-done.3
  297.1 2.9 convolution_convert_fusion
  300.2 19.0 %all_to_all.27 = bf16[4,512,512]{2,1,0:T(8,128)(2,1)S(1)} all-to-all(bf16[4,512,512]{2,1,0:T(8,128)(2,1)S(1)} %bitcast.291), channel_id=1, replica_groups=mesh['sp_0'=8,'sp_1'=8,'sp_2'=2,'tp'=4] {'tp'}, dimensions={0} | all-to-all | bytes 4194304 | tf_op jit(solution)/shard_map/all_to_all | solution.py:88
  319.2 1.2 reduce_sum.52
  (239 shorter events, 11.6 us)
Async XLA Ops:
  6.5 288.8 %copy-start = (bf16[1,256,256]{2,1,0:T(8,128)(2,1)S(1)}, bf16[1,256,256]{2,1,0:T(8,128)(2,1)}, u32[]{:S(2)}) copy-start(bf16[1,256,256]{2,1,0:T(8,128)(2,1)} %param.30) | copy-start | bytes 393220
  8.4 13.0 %all-to-all-start = ((f32[4,1,512]{2,1,0:T(1,128)}), f32[4,1,512]{2,1,0:T(1,128)S(1)}, u32[]{:S(2)}, u32[]{:S(2)}) async-start(f32[4,1,512]{2,1,0:T(1,128)} %broadcast_in_dim.62), calls=%async_computation | async-start | bytes 16384 | tf_op jit(solution)/shard_map/all_to_all | solution.py:19
  24.4 5.2 %copy-start.65 = (bf16[16,4]{0,1:T(4,128)(2,1)S(1)}, bf16[16,4]{0,1:T(4,128)(2,1)}, u32[]{:S(2)}) copy-start(bf16[16,4]{0,1:T(4,128)(2,1)} %param.29) | copy-start | bytes 388
  24.4 5.3 %copy-start.28 = (bf16[16,256]{1,0:T(8,128)(2,1)S(1)}, bf16[16,256]{1,0:T(8,128)(2,1)}, u32[]{:S(2)}) copy-start(bf16[16,256]{1,0:T(8,128)(2,1)} %param.24) | copy-start | bytes 24580
  24.4 5.3 %copy-start.29 = (bf16[16,256]{1,0:T(8,128)(2,1)S(1)}, bf16[16,256]{1,0:T(8,128)(2,1)}, u32[]{:S(2)}) copy-start(bf16[16,256]{1,0:T(8,128)(2,1)} %param.25) | copy-start | bytes 24580
  24.4 5.3 %copy-start.30 = (bf16[16,256]{1,0:T(8,128)(2,1)S(1)}, bf16[16,256]{1,0:T(8,128)(2,1)}, u32[]{:S(2)}) copy-start(bf16[16,256]{1,0:T(8,128)(2,1)} %param.26) | copy-start | bytes 24580
  24.4 5.3 %copy-start.50 = (bf16[16,64]{1,0:T(8,128)(2,1)S(1)}, bf16[16,64]{1,0:T(8,128)(2,1)}, u32[]{:S(2)}) copy-start(bf16[16,64]{1,0:T(8,128)(2,1)} %param.27) | copy-start | bytes 6148
  24.4 5.3 %copy-start.51 = (bf16[16,64]{1,0:T(8,128)(2,1)S(1)}, bf16[16,64]{1,0:T(8,128)(2,1)}, u32[]{:S(2)}) copy-start(bf16[16,64]{1,0:T(8,128)(2,1)} %param.28) | copy-start | bytes 6148
  24.4 24.6 %all-to-all-start.1 = ((bf16[4,512,512]{1,2,0:T(8,128)(2,1)}), bf16[4,512,512]{1,2,0:T(8,128)(2,1)S(1)}, u32[]{:S(2)}, u32[]{:S(2)}) async-start(bf16[4,512,512]{1,2,0:T(8,128)(2,1)} %broadcast_in_dim.63), calls=%async_computation.1 | async-start | bytes 4194304 | tf_op jit(solution)/shard_map/all_to_all | solution.py:19
  51.6 18.6 %copy-start.31 = (bf16[256,16]{0,1:T(8,128)(2,1)S(1)}, bf16[256,16]{0,1:T(8,128)(2,1)}, u32[]{:S(2)}) copy-start(bf16[256,16]{0,1:T(8,128)(2,1)} %param.41) | copy-start | bytes 24580
  51.6 18.6 %copy-start.32 = (bf16[256,16]{0,1:T(8,128)(2,1)S(1)}, bf16[256,16]{0,1:T(8,128)(2,1)}, u32[]{:S(2)}) copy-start(bf16[256,16]{0,1:T(8,128)(2,1)} %param.40) | copy-start | bytes 24580
  51.6 19.3 %copy-start.67 = (f32[4]{0:T(128)S(1)}, f32[4]{0:T(128)}, u32[]{:S(2)}) copy-start(f32[4]{0:T(128)} %param.38) | copy-start | bytes 52
  51.6 20.7 %copy-start.52 = (f32[4,256]{1,0:T(4,128)S(1)}, f32[4,256]{1,0:T(4,128)}, u32[]{:S(2)}) copy-start(f32[4,256]{1,0:T(4,128)} %param.32) | copy-start | bytes 12292
  51.6 20.7 %copy-start.60 = (f32[4,64]{1,0:T(4,128)S(1)}, f32[4,64]{1,0:T(4,128)}, u32[]{:S(2)}) copy-start(f32[4,64]{1,0:T(4,128)} %param.34) | copy-start | bytes 3076
  51.6 20.7 %copy-start.61 = (f32[4,64]{1,0:T(4,128)S(1)}, f32[4,64]{1,0:T(4,128)}, u32[]{:S(2)}) copy-start(f32[4,64]{1,0:T(4,128)} %param.33) | copy-start | bytes 3076
  51.6 22.0 %copy-start.69 = (f32[4]{0:T(128)S(1)}, f32[4]{0:T(128)}, u32[]{:S(2)}) copy-start(f32[4]{0:T(128)} %param.36) | copy-start | bytes 52
  51.6 115.2 %all-to-all-start.2 = ((bf16[128,16,900]{2,1,0:T(8,128)(2,1)}), bf16[128,16,900]{2,1,0:T(8,128)(2,1)}, u32[]{:S(2)}, u32[]{:S(2)}) async-start(bf16[128,16,900]{2,1,0:T(8,128)(2,1)} %stack.12), calls=%async_computation.2 | async-start | bytes 8388608 | tf_op jit(solution)/shard_map/all_to_all | solution.py:138
  70.1 227.0 %all-gather.8.cloned.1.call-start = ((), (), s32[]{:S(2)}) async-start(), calls=%async_computation.5 | async-start | bytes 2113536 | tf_op jit(solution)/shard_map/all_gather | solution.py:253
  166.8 4.4 %copy-start.33 = (f32[512,4]{0,1:T(4,128)S(1)}, f32[512,4]{0,1:T(4,128)}, u32[]{:S(2)}) copy-start(f32[512,4]{0,1:T(4,128)} %param.37) | copy-start | bytes 24580
  166.8 4.4 %copy-start.66 = (f32[4]{0:T(128)S(1)}, f32[4]{0:T(128)}, u32[]{:S(2)}) copy-start(f32[4]{0:T(128)} %param.35) | copy-start | bytes 52
  171.9 11.5 %copy-start.24 = (f32[384]{0:T(512)S(1)}, f32[384]{0:T(512)}, u32[]{:S(2)}) copy-start(f32[384]{0:T(512)} %get-tuple-element.53) | copy-start | bytes 4612
  171.9 11.5 %copy-start.25 = (f32[384]{0:T(512)S(1)}, f32[384]{0:T(512)}, u32[]{:S(2)}) copy-start(f32[384]{0:T(512)} %get-tuple-element.54) | copy-start | bytes 4612
  171.9 11.5 %copy-start.26 = (f32[384]{0:T(512)S(1)}, f32[384]{0:T(512)}, u32[]{:S(2)}) copy-start(f32[384]{0:T(512)} %get-tuple-element.55) | copy-start | bytes 4612
  171.9 11.5 %copy-start.27 = (f32[384]{0:T(512)S(1)}, f32[384]{0:T(512)}, u32[]{:S(2)}) copy-start(f32[384]{0:T(512)} %get-tuple-element.56) | copy-start | bytes 4612
  172.0 11.2 %collective-permute-start.1 = (bf16[3,384]{0,1:T(8,128)(2,1)S(1)}, bf16[3,384]{0,1:T(8,128)(2,1)S(1)}, u32[]{:S(2)}, u32[]{:S(2)}) collective-permute-start(bf16[3,384]{0,1:T(8,128)(2,1)S(1)} %slice.368), channel_id=1, source_target_pairs={{0,4},{4,8},{8,12},{12,16},{16,20},{20,24},{24,28},{28,32},{32,36}... | collective-permute-start | bytes 6920 | tf_op jit(solution)/shard_map/ppermute | solution.py:40
  176.5 116.6 %collective-permute-start = (bf16[15,256]{0,1:T(8,128)(2,1)}, bf16[15,256]{0,1:T(8,128)(2,1)}, u32[]{:S(2)}, u32[]{:S(2)}) collective-permute-start(bf16[15,256]{0,1:T(8,128)(2,1)} %slice.355), channel_id=1, source_target_pairs={{0,4},{4,8},{8,12},{12,16},{16,20},{20,24},{24,28},{28,32},{32,36}... | collective-permute-start | bytes 23048 | tf_op jit(solution)/shard_map/ppermute | solution.py:40
  191.6 28.9 %copy-start.48 = (f32[4]{0:T(128)}, f32[4]{0:T(128)S(1)}, u32[]{:S(2)}) copy-start(f32[4]{0:T(128)S(1)} %get-tuple-element.116) | copy-start | bytes 52
  191.6 28.9 %copy-start.63 = (f32[4]{0:T(128)}, f32[4]{0:T(128)S(1)}, u32[]{:S(2)}) copy-start(f32[4]{0:T(128)S(1)} %get-tuple-element.117) | copy-start | bytes 52
  220.5 2.0 copy-start.34
  264.3 14.3 %copy-start.4 = (f32[8,4,8,128]{3,2,1,0:T(8,128)S(1)}, f32[8,4,8,128]{3,2,1,0:T(8,128)}, u32[]{:S(2)}) copy-start(f32[8,4,8,128]{3,2,1,0:T(8,128)} %get-tuple-element.93) | copy-start | bytes 393220
  265.1 14.6 %copy-start.1 = (f32[4,4,64,64]{3,2,1,0:T(8,128)S(1)}, f32[4,4,64,64]{3,2,1,0:T(8,128)}, u32[]{:S(2)}) copy-start(f32[4,4,64,64]{3,2,1,0:T(8,128)} %get-tuple-element.33) | copy-start | bytes 786436
  265.1 15.9 %copy-start.3 = (f32[8,4,8,128]{3,2,0,1:T(8,128)S(1)}, f32[8,4,8,128]{3,2,0,1:T(8,128)}, u32[]{:S(2)}) copy-start(f32[8,4,8,128]{3,2,0,1:T(8,128)} %copy-done.2) | copy-start | bytes 393220
  271.4 12.3 %copy-start.5 = (f32[1,256,64]{2,1,0:T(8,128)S(1)}, f32[1,256,64]{2,1,0:T(8,128)}, u32[]{:S(2)}) copy-start(f32[1,256,64]{2,1,0:T(8,128)} %copy.267) | copy-start | bytes 196612
  271.4 12.3 %copy-start.6 = (f32[1,256,64]{2,1,0:T(8,128)S(1)}, f32[1,256,64]{2,1,0:T(8,128)}, u32[]{:S(2)}) copy-start(f32[1,256,64]{2,1,0:T(8,128)} %copy.268) | copy-start | bytes 196612
  276.0 7.7 %copy-start.23 = (f32[4,128,4]{1,2,0:T(4,128)S(1)}, f32[4,128,4]{1,2,0:T(4,128)}, u32[]{:S(2)}) copy-start(f32[4,128,4]{1,2,0:T(4,128)} %copy.260) | copy-start | bytes 24580
  276.1 7.7 %copy-start.35 = (f32[4]{0:T(128)S(1)}, f32[4]{0:T(128)}, u32[]{:S(2)}) copy-start(f32[4]{0:T(128)} %copy-done.34) | copy-start | bytes 52
  276.1 7.7 %copy-start.37 = (f32[4]{0:T(128)S(1)}, f32[4]{0:T(128)}, u32[]{:S(2)}) copy-start(f32[4]{0:T(128)} %copy-done.36) | copy-start | bytes 52
  276.1 7.8 %copy-start.39 = (f32[4]{0:T(128)S(1)}, f32[4]{0:T(128)}, u32[]{:S(2)}) copy-start(f32[4]{0:T(128)} %copy-done.38) | copy-start | bytes 52
  276.1 7.8 %copy-start.41 = (f32[4]{0:T(128)S(1)}, f32[4]{0:T(128)}, u32[]{:S(2)}) copy-start(f32[4]{0:T(128)} %copy-done.40) | copy-start | bytes 52
  276.1 7.8 %copy-start.43 = (f32[4]{0:T(128)S(1)}, f32[4]{0:T(128)}, u32[]{:S(2)}) copy-start(f32[4]{0:T(128)} %copy-done.42) | copy-start | bytes 52
  276.1 7.8 %copy-start.45 = (f32[4]{0:T(128)S(1)}, f32[4]{0:T(128)}, u32[]{:S(2)}) copy-start(f32[4]{0:T(128)} %copy-done.44) | copy-start | bytes 52
  276.1 7.8 %copy-start.47 = (f32[4]{0:T(128)S(1)}, f32[4]{0:T(128)}, u32[]{:S(2)}) copy-start(f32[4]{0:T(128)} %copy-done.46) | copy-start | bytes 52
  276.1 7.8 %copy-start.49 = (f32[4]{0:T(128)S(1)}, f32[4]{0:T(128)}, u32[]{:S(2)}) copy-start(f32[4]{0:T(128)} %copy-done.48) | copy-start | bytes 52
  276.1 7.8 %copy-start.55 = (f32[4]{0:T(128)S(1)}, f32[4]{0:T(128)}, u32[]{:S(2)}) copy-start(f32[4]{0:T(128)} %copy-done.54) | copy-start | bytes 52
  276.1 7.8 %copy-start.57 = (f32[4]{0:T(128)S(1)}, f32[4]{0:T(128)}, u32[]{:S(2)}) copy-start(f32[4]{0:T(128)} %copy-done.56) | copy-start | bytes 52
  276.1 7.8 %copy-start.58 = (f32[4]{0:T(128)S(1)}, f32[4]{0:T(128)}, u32[]{:S(2)}) copy-start(f32[4]{0:T(128)} %get-tuple-element.69) | copy-start | bytes 52
  276.1 7.8 %copy-start.59 = (f32[4]{0:T(128)S(1)}, f32[4]{0:T(128)}, u32[]{:S(2)}) copy-start(f32[4]{0:T(128)} %get-tuple-element.70) | copy-start | bytes 52
  278.5 5.4 %copy-start.7 = (f32[1,256,64]{2,1,0:T(8,128)S(1)}, f32[1,256,64]{2,1,0:T(8,128)}, u32[]{:S(2)}) copy-start(f32[1,256,64]{2,1,0:T(8,128)} %copy.269) | copy-start | bytes 196612
  278.5 5.4 %copy-start.8 = (f32[1,256,64]{2,1,0:T(8,128)S(1)}, f32[1,256,64]{2,1,0:T(8,128)}, u32[]{:S(2)}) copy-start(f32[1,256,64]{2,1,0:T(8,128)} %copy.270) | copy-start | bytes 196612
  278.5 5.4 %copy-start.9 = (f32[1,256,64]{2,1,0:T(8,128)S(1)}, f32[1,256,64]{2,1,0:T(8,128)}, u32[]{:S(2)}) copy-start(f32[1,256,64]{2,1,0:T(8,128)} %copy.271) | copy-start | bytes 196612
  278.5 5.4 %copy-start.10 = (f32[1,256,64]{2,1,0:T(8,128)S(1)}, f32[1,256,64]{2,1,0:T(8,128)}, u32[]{:S(2)}) copy-start(f32[1,256,64]{2,1,0:T(8,128)} %copy.272) | copy-start | bytes 196612
  278.5 5.4 %copy-start.11 = (f32[1,256,64]{2,1,0:T(8,128)S(1)}, f32[1,256,64]{2,1,0:T(8,128)}, u32[]{:S(2)}) copy-start(f32[1,256,64]{2,1,0:T(8,128)} %copy.273) | copy-start | bytes 196612
  278.5 5.4 %copy-start.12 = (f32[1,256,64]{2,1,0:T(8,128)S(1)}, f32[1,256,64]{2,1,0:T(8,128)}, u32[]{:S(2)}) copy-start(f32[1,256,64]{2,1,0:T(8,128)} %copy.274) | copy-start | bytes 196612
  278.5 5.4 %copy-start.13 = (f32[1,256,64]{2,1,0:T(8,128)S(1)}, f32[1,256,64]{2,1,0:T(8,128)}, u32[]{:S(2)}) copy-start(f32[1,256,64]{2,1,0:T(8,128)} %copy.275) | copy-start | bytes 196612
  278.6 5.4 %copy-start.14 = (f32[1,256,64]{2,1,0:T(8,128)S(1)}, f32[1,256,64]{2,1,0:T(8,128)}, u32[]{:S(2)}) copy-start(f32[1,256,64]{2,1,0:T(8,128)} %copy.276) | copy-start | bytes 196612
  278.6 5.4 %copy-start.15 = (f32[1,256,64]{2,1,0:T(8,128)S(1)}, f32[1,256,64]{2,1,0:T(8,128)}, u32[]{:S(2)}) copy-start(f32[1,256,64]{2,1,0:T(8,128)} %copy.277) | copy-start | bytes 196612
  278.6 5.4 %copy-start.16 = (f32[1,256,64]{2,1,0:T(8,128)S(1)}, f32[1,256,64]{2,1,0:T(8,128)}, u32[]{:S(2)}) copy-start(f32[1,256,64]{2,1,0:T(8,128)} %copy.278) | copy-start | bytes 196612
  278.6 5.4 %copy-start.17 = (f32[1,256,64]{2,1,0:T(8,128)S(1)}, f32[1,256,64]{2,1,0:T(8,128)}, u32[]{:S(2)}) copy-start(f32[1,256,64]{2,1,0:T(8,128)} %copy.279) | copy-start | bytes 196612
  278.6 5.4 %copy-start.18 = (f32[1,256,64]{2,1,0:T(8,128)S(1)}, f32[1,256,64]{2,1,0:T(8,128)}, u32[]{:S(2)}) copy-start(f32[1,256,64]{2,1,0:T(8,128)} %copy.280) | copy-start | bytes 196612
  278.6 5.4 %copy-start.19 = (f32[1,256,64]{2,1,0:T(8,128)S(1)}, f32[1,256,64]{2,1,0:T(8,128)}, u32[]{:S(2)}) copy-start(f32[1,256,64]{2,1,0:T(8,128)} %copy.281) | copy-start | bytes 196612
  278.6 5.4 %copy-start.20 = (f32[1,256,64]{2,1,0:T(8,128)S(1)}, f32[1,256,64]{2,1,0:T(8,128)}, u32[]{:S(2)}) copy-start(f32[1,256,64]{2,1,0:T(8,128)} %copy.282) | copy-start | bytes 196612
  278.6 5.4 %copy-start.21 = (f32[1,256,64]{2,1,0:T(8,128)S(1)}, f32[1,256,64]{2,1,0:T(8,128)}, u32[]{:S(2)}) copy-start(f32[1,256,64]{2,1,0:T(8,128)} %copy.283) | copy-start | bytes 196612
  278.6 5.4 %copy-start.22 = (f32[1,256,64]{2,1,0:T(8,128)S(1)}, f32[1,256,64]{2,1,0:T(8,128)}, u32[]{:S(2)}) copy-start(f32[1,256,64]{2,1,0:T(8,128)} %copy.284) | copy-start | bytes 196612
  287.3 9.6 %all-to-all-start.3 = ((f32[4,1,512]{2,1,0:T(1,128)}), f32[4,1,512]{2,1,0:T(1,128)S(1)}, u32[]{:S(2)}, u32[]{:S(2)}) async-start(f32[4,1,512]{2,1,0:T(1,128)} %broadcast_in_dim.73), calls=%async_computation.3 | async-start | bytes 16384 | tf_op jit(solution)/shard_map/all_to_all | solution.py:19
  (13 other events, 19.4 us)
Sparse Core Ops, SparseCore 0:
  74.0 150.9 all-gather.7
